TPU v7x, 32 devices: a whole 2x2x4 slice. The times are simulated.
32 devices in a mesh: grp: 2 (over y), sp: 4 (over z), tp: 4 (over x, core).
Axes of the slice: x: 2, y: 2, z: 4, core: 2. Of those that a mesh axis runs over, the one named last changes fastest.
Arguments:
- layer_input: bfloat16 [8, 1536, 2048], P(('grp', 'tp'), 'sp'), parts along dimension 0, may hold values from -6 to 6
- input_gain: float32 [2048], replicated, may hold values from 0.1 to 1.9
- key_weight: bfloat16 [2048, 512], replicated, may hold values from -0.125 to 0.125
- value_weight: bfloat16 [2048, 512], replicated, may hold values from -0.125 to 0.125
- stick_offsets: bfloat16 [4, 8, 1536], P(None, ('grp', 'tp'), 'sp'), parts along dimension 1
- head_bias: float32 [16], replicated
- queries: bfloat16 [8, 4, 512], P(('grp', 'tp'), 'sp'), parts along dimension 0, may hold values from -6 to 6
Outputs:
- key_cache: bfloat16 [8, 4, 1536, 128], P(('grp', 'tp'), 'sp'), parts along dimension 0
- value_cache: bfloat16 [8, 4, 1536, 128], P(('grp', 'tp'), 'sp'), parts along dimension 0
- offset_cache: bfloat16 [8, 4, 1536], P(('grp', 'tp'), 'sp'), parts along dimension 0
- first_read: bfloat16 [8, 4, 512], P(('grp', 'tp'), 'sp'), parts along dimension 0
There are 2 independent parts, one for each index of `grp`. A program takes and returns all parts, laid end to end along the dimension named above; an argument that names none is the same for every part. Nothing has to cross between parts.
All inputs are finite; a program needn't handle non-finite values.
Results may differ from a plain program's by a relative error of at most 0.014.
Values may be sent and summed in bfloat16 or wider, within the bound.
A program may use at most 64 MiB of HBM per device.

v0:
```python
import functools
import math

import jax
import jax.numpy as jnp
from jax import lax
from jax.experimental import pallas as pl
from jax.experimental.pallas import tpu as pltpu
from jax.sharding import PartitionSpec as P

H = 16
KVH = 4
HD = 128
EPSILON = 1e-06
ROWS = 128
PIECES = 4
VMEM_BYTES = 67043328
SPARE_BYTES = 262144
WRITE_BYTES = 1048576
MESH = pl.DeviceIdType.MESH


def kernel(
    n, seqs, x_hbm, gain_ref, wk_hbm, wv_hbm, off_hbm, bias_ref, q_hbm,
    k_land, v_land, off_out, read_out,
    x_buf, normed, weights, sends, off_in, off_send, off_land, q_buf, stick,
    x_sem, w_sem, small_sem, k_sem, v_sem, o_sem,
):
    total, width = x_buf.shape
    block = total // seqs
    length = n * block
    group = H // KVH
    me = lax.axis_index("sp")
    order = range(1, n)
    paired = jnp.minimum(me, n - 1 - me)
    toward = jnp.where(2 * me < n, 1, -1)

    def peer(i):
        near = me + toward * (1 if i % 2 else -1) * ((i + 1) // 2)
        far = me + toward * (i - paired)
        return jnp.where(i <= 2 * paired, near, far) if i else me

    def offset(i):
        return lax.rem(peer(i) - me + n, n)

    def source(d):
        return lax.rem(me + n - d, n)

    def columns(i):
        return pl.ds(pl.multiple_of(lax.rem(peer(i), KVH) * HD, HD), HD)

    x_copies = []
    for c in range(total // ROWS):
        part = pl.ds(c * ROWS, ROWS)
        x_copies.append(pltpu.make_async_copy(x_hbm.at[part], x_buf.at[part], x_sem.at[c]))
    w_copies = {}
    for kind, w_hbm in enumerate((wk_hbm, wv_hbm)):
        for j in range(PIECES):
            part = pl.ds(j * (width // PIECES), width // PIECES)
            w_copies[kind, j] = pltpu.make_async_copy(
                w_hbm.at[part], weights.at[kind, part], w_sem.at[kind, j]
            )
    x_copies[0].start()
    for j in range(PIECES):
        w_copies[0, j].start()
    for copy in x_copies[1:]:
        copy.start()
    for j in range(PIECES):
        w_copies[1, j].start()
    off_copy = pltpu.make_async_copy(off_hbm, off_in, small_sem.at[0])
    off_copy.start()
    q_copy = pltpu.make_async_copy(q_hbm, q_buf, small_sem.at[1])
    q_copy.start()

    barrier = pltpu.get_barrier_semaphore()
    for d in order:
        pl.semaphore_signal(barrier, inc=1, device_id={"sp": source(d)}, device_id_type=MESH)

    gain = gain_ref[...]
    step_rows = 16
    def norm(c):
        x_copies[c].wait()

        def norm_step(i, _):
            rows = pl.ds(pl.multiple_of(c * ROWS + i * step_rows, step_rows), step_rows)
            x = x_buf[rows, :].astype(jnp.float32)
            scale = lax.rsqrt(jnp.mean(x * x, axis=-1, keepdims=True) + EPSILON)
            normed[rows, :] = (x * scale * gain).astype(jnp.bfloat16)
            return 0

        lax.fori_loop(0, ROWS // step_rows, norm_step, 0, unroll=4)

    def wait_weights(kind):
        for j in range(PIECES):
            w_copies[kind, j].wait()

    def project(kind, i, dst):
        if i == 1:
            wait_weights(kind)
        if seqs == 1:
            rows = normed[...]
        else:
            base = lax.div(peer(i), KVH) * block
            rows = normed[pl.ds(pl.multiple_of(base, 16), block), :]
        dst[...] = jnp.dot(
            rows, weights[kind, :, columns(i)], preferred_element_type=jnp.float32
        ).astype(jnp.bfloat16)

    def remote(src, dst, sem, d, target):
        return pltpu.make_async_remote_copy(
            src_ref=src, dst_ref=dst, send_sem=sem.at[0, d], recv_sem=sem.at[1, d],
            device_id={"sp": target}, device_id_type=MESH,
        )

    here = pl.ds(pl.multiple_of(me * block, block), block)

    def block_copy(kind, i):
        land, sem = ((k_land, k_sem), (v_land, v_sem))[kind]
        return remote(sends.at[kind, i], land.at[0, 0, here], sem, offset(i), peer(i))

    def offset_copy(i):
        return remote(off_send.at[peer(i)], off_land.at[me], o_sem, offset(i), peer(i))

    if seqs == 1:
        for c in range(total // ROWS):
            norm(c)
            if c == 0:
                wait_weights(0)
            part = pl.ds(c * ROWS, ROWS)
            sends[0, 1, part] = jnp.dot(
                normed[part, :], weights[0, :, columns(1)], preferred_element_type=jnp.float32
            ).astype(jnp.bfloat16)
            if c == 0:
                pl.semaphore_wait(barrier, n - 1)
            there = pl.ds(pl.multiple_of(me * block + c * ROWS, ROWS), ROWS)
            remote(
                sends.at[0, 1, part], k_land.at[0, 0, there], k_sem, offset(1), peer(1)
            ).start()
    else:
        for c in range(total // ROWS):
            norm(c)
    for i in order:
        if seqs > 1 or i > 1:
            project(0, i, sends.at[0, i])
            if i == 1:
                pl.semaphore_wait(barrier, n - 1)
            block_copy(0, i).start()
        if i == 1:
            off_copy.wait()
            for s in range(seqs):
                values = off_in[s].astype(jnp.float32)
                for h in range(KVH):
                    off_send[s * KVH + h] = values[h:h + 1, :]
            off_land[me] = off_send[me]
    for i in order:
        offset_copy(i).start()
    for i in order:
        project(1, i, sends.at[1, i])
        block_copy(1, i).start()
    project(0, 0, k_land.at[0, 0, here])
    project(1, 0, v_land.at[0, 0, here])

    def rows_of(i):
        return pl.ds(pl.multiple_of(peer(i) * block, block), block)

    def arrived(src, land, sem, i):
        d = lax.rem(me - peer(i) + n, n)
        remote(src, land.at[0, 0, rows_of(i)], sem, d, peer(i)).wait_recv()

    q_copy.wait()
    q_all = q_buf[0].astype(jnp.float32)
    q_rows = jnp.concatenate([q_all[:, g * HD:(g + 1) * HD] for g in range(group)] * 2, axis=0)
    q_rows = q_rows.astype(jnp.bfloat16)
    for d in order:
        remote(off_send.at[0], off_land.at[source(d)], o_sem, d, source(d)).wait_recv()
    off_row = jnp.concatenate([off_land[i] for i in range(n)], axis=1)
    off_out[0] = off_row.astype(jnp.bfloat16)
    head = lax.rem(me, KVH)
    row_id = lax.broadcasted_iota(jnp.int32, (2 * group, 1), 0)
    bias = jnp.zeros((2 * group, 1), jnp.float32)
    for g in range(group):
        value = bias_ref[head * group + g]
        bias = jnp.where((row_id == g) | (row_id == g + group), value, bias)
    for d in order:
        arrived(sends.at[0, d], k_land, k_sem, d)
    scores = lax.dot_general(
        q_rows, k_land[0, 0], (((1,), (1,)), ((), ())), preferred_element_type=jnp.float32
    )
    scores = scores / math.sqrt(HD) + bias + off_row
    tail = jnp.log1p(jnp.exp(-jnp.abs(scores)))
    spread = jnp.maximum(scores, 0.0) + tail
    log_sig = jnp.minimum(scores, 0.0) - tail
    chunks = length // HD
    cut = [spread[:, c * HD:(c + 1) * HD] for c in range(chunks)]
    stacked = jnp.concatenate(cut, axis=0)
    after = (
        lax.broadcasted_iota(jnp.int32, (HD, HD), 0) > lax.broadcasted_iota(jnp.int32, (HD, HD), 1)
    ).astype(jnp.float32)
    inner = jnp.dot(
        stacked, after, preferred_element_type=jnp.float32, precision=lax.Precision.HIGHEST
    )
    sums = jnp.sum(stacked, axis=1, keepdims=True)
    carried = jnp.zeros((2 * group, 1), jnp.float32)
    for c in reversed(range(chunks)):
        rows = slice(c * 2 * group, (c + 1) * 2 * group)
        beyond = inner[rows] + carried
        stick[:, c * HD:(c + 1) * HD] = jnp.exp(log_sig[:, c * HD:(c + 1) * HD] - beyond)
        carried = carried + sums[rows]

    mixture = jnp.zeros((2 * group, HD), jnp.float32)
    for d in range(n):
        if d:
            arrived(sends.at[1, d], v_land, v_sem, d)
        part = rows_of(d)
        mixture = mixture + jnp.dot(
            stick[:, part].astype(jnp.bfloat16), v_land[0, 0, part, :], preferred_element_type=jnp.float32
        )
    scale = lax.rsqrt(jnp.mean(mixture * mixture, axis=-1, keepdims=True) + EPSILON)
    read = mixture * scale
    read_out[0] = jnp.concatenate([read[g:g + 1] for g in range(group)], axis=1).astype(jnp.bfloat16)

    for i in order:
        block_copy(0, i).wait_send()
        block_copy(1, i).wait_send()
        offset_copy(i).wait_send()


def write_out(*refs):
    *refs, sem = refs
    half = len(refs) // 2
    copies = [
        pltpu.make_async_copy(refs[i], refs[half + i], sem.at[i]) for i in range(half)
    ]
    for copy in copies:
        copy.start()
    for copy in copies:
        copy.wait()


def shards(layer_input, input_gain, key_weight, value_weight, stick_offsets, head_bias, queries):
    seqs, block, width = layer_input.shape
    n = lax.axis_size("sp")
    length = n * block
    total = seqs * block
    hbm = pl.BlockSpec(memory_space=pltpu.HBM)
    vmem = pl.BlockSpec(memory_space=pltpu.VMEM)
    smem = pl.BlockSpec(memory_space=pltpu.SMEM)
    group_width = queries.shape[-1]
    outs = (
        ((1, 1, length, HD), jnp.bfloat16),
        ((1, 1, length, HD), jnp.bfloat16),
        ((1, 1, length), jnp.bfloat16),
        ((1, 1, group_width), jnp.bfloat16),
    )
    held = pl.pallas_call(
        functools.partial(kernel, n, seqs),
        out_shape=tuple(pltpu.VMEM(*out) for out in outs),
        in_specs=[hbm, vmem, hbm, hbm, hbm, smem, hbm],
        out_specs=(vmem, vmem, vmem, vmem),
        scratch_shapes=[
            pltpu.VMEM((total, width), jnp.bfloat16),
            pltpu.VMEM((total, width), jnp.bfloat16),
            pltpu.VMEM((2, width, KVH * HD), jnp.bfloat16),
            pltpu.VMEM((2, n, block, HD), jnp.bfloat16),
            pltpu.VMEM((seqs, KVH, block), jnp.bfloat16),
            pltpu.VMEM((n, 1, block), jnp.float32),
            pltpu.VMEM((n, 1, block), jnp.float32),
            pltpu.VMEM((1, 1, group_width), jnp.bfloat16),
            pltpu.VMEM((2 * (H // KVH), length), jnp.float32),
            pltpu.SemaphoreType.DMA((total // ROWS,)),
            pltpu.SemaphoreType.DMA((2, PIECES)),
            pltpu.SemaphoreType.DMA((2,)),
            pltpu.SemaphoreType.DMA((2, n)),
            pltpu.SemaphoreType.DMA((2, n)),
            pltpu.SemaphoreType.DMA((2, n)),
        ],
        compiler_params=pltpu.CompilerParams(
            collective_id=0, has_side_effects=True, vmem_limit_bytes=VMEM_BYTES - 4 * length * HD - SPARE_BYTES
        ),
    )(
        layer_input.reshape(total, width),
        input_gain.reshape(1, width),
        key_weight,
        value_weight,
        jnp.transpose(stick_offsets, (1, 0, 2)),
        head_bias,
        queries,
    )
    return pl.pallas_call(
        write_out,
        out_shape=tuple(jax.ShapeDtypeStruct(*out) for out in outs),
        in_specs=[vmem] * len(outs),
        out_specs=(hbm,) * len(outs),
        scratch_shapes=[pltpu.SemaphoreType.DMA((len(outs),))],
        compiler_params=pltpu.CompilerParams(vmem_limit_bytes=WRITE_BYTES),
    )(*held)


def solution(mesh):
    placed = (
        P(("grp", "tp"), "sp", None),
        P(),
        P(),
        P(),
        P(None, ("grp", "tp"), "sp"),
        P(),
        P(("grp", "tp"), "sp", None),
    )
    return jax.shard_map(
        shards,
        mesh=mesh,
        in_specs=placed,
        out_specs=(
            P(("grp", "tp"), "sp", None, None),
            P(("grp", "tp"), "sp", None, None),
            P(("grp", "tp"), "sp", None),
            P(("grp", "tp"), "sp", None),
        ),
        check_vma=False,
    )
```

profile of v0, /device:TPU:0, one launch (start us, length us, event | category | flops | bytes accessed | tf_op | source)
XLA Modules:
  0.0 28.2 jit_solution(15559168223507740681)
XLA Ops:
  0.6 26.6 %shard_map.102 = (bf16[1,1,1536,128]{3,2,1,0:T(8,128)(2,1)S(1)}, bf16[1,1,1536,128]{3,2,1,0:T(8,128)(2,1)S(1)}, bf16[1,1,1536]{2,1,0:T(2,128)(2,1)S(1)}, bf16[1,1,512]{2,1,0:T(2,128)(2,1)S(1)}) custom-call(bf16[384,2048]{1,0:T(8,128)(2,1)} %bitcast.3, f32[1,2048]{1,0:T(1,128)} %bitcast.4, bf16[2048,512]{1,0:T(8,128)(2,1)} %wk_hbm.1, ...), custom_call_target="tpu_custom_call" | custom-call | tf_op jit(solution)/shard_map/pallas_call | solution.py:255
  27.3 0.9 %shard_map.103 = (bf16[1,1,1536,128]{3,2,1,0:T(8,128)(2,1)}, bf16[1,1,1536,128]{3,2,1,0:T(8,128)(2,1)}, bf16[1,1,1536]{2,1,0:T(2,128)(2,1)}, bf16[1,1,512]{2,1,0:T(2,128)(2,1)}) custom-call(bf16[1,1,1536,128]{3,2,1,0:T(8,128)(2,1)S(1)} %get-tuple-element.8.refs_0_, bf16[1,1,1536,128]{3,2,1,0:T(8,128)(2,1)S(1)} %get-tuple-element.9.refs_1_, ...), custom_call_target="tpu_custom_call" | custom-call | tf_op jit(solution)/shard_map/pallas_call | solution.py:289
where the time goes:
time: 28.4 us; the launch traced here: 28.2 us
  Pallas kernels  27.5 us (97%)
  between operations  0.64 us (2%)
    pallas_call x1, Pallas kernels, shards(): pl.pallas_call(functools.partial(kernel, n, seqs), out_shape=tuple((pltpu...  26.6 us
    pallas_call x1, Pallas kernels, shards(): pl.pallas_call(write_out, out_shape=tuple((jax.ShapeDtypeStruct(*out) for...  0.92 us

commit v1 on v0

v1 whole, which is shorter than its diff:
```python
import functools
import math

import jax
import jax.numpy as jnp
from jax import lax
from jax.experimental import pallas as pl
from jax.experimental.pallas import tpu as pltpu
from jax.sharding import PartitionSpec as P

H = 16
KVH = 4
HD = 128
GROUP = H // KVH
EPSILON = 1e-06
ROWS = 128
FIRST = 64
STEP = 16
VMEM_BYTES = 67043328
SPARE_BYTES = 524288
WRITE_BYTES = 1048576
MESH = pl.DeviceIdType.MESH


def last_source(me, n):
    return jnp.where(2 * me < n, n // 2, n // 2 - 1)


def kernel(
    n, seqs, chunks, x_hbm, gain_hbm, wk_hbm, wv_hbm, off_hbm, bias_hbm, q_hbm,
    k_land, v_land, off_out, stick, mix_out,
    x_buf, scaled, row_scale, weights, sends, gain_buf, bias_buf, off_in, off_send, off_land, q_buf,
    x_sem, w_sem, small_sem, k_sem, v_sem, o_sem,
):
    total, width = x_buf.shape
    block = total // seqs
    length = n * block
    me = lax.axis_index("sp")
    order = range(1, n)
    lower = 2 * me < n
    near = jnp.where(lower, me, n - 1 - me)

    barrier = pltpu.get_barrier_semaphore()
    for d in order:
        pl.semaphore_signal(
            barrier, inc=1, device_id={"sp": lax.rem(me + d, n)}, device_id_type=MESH
        )

    def peer(i):
        if i == 0:
            return me
        far = jnp.where(i <= n - 1 - near, n - i, n - 1 - i)
        return jnp.where(lower, far, n - 1 - far)

    def offset(i):
        return lax.rem(peer(i) - me + n, n)

    def head_of(i):
        return lax.rem(peer(i), KVH)

    x_copies = []
    for c, (start, rows) in enumerate(chunks):
        part = pl.ds(start, rows)
        x_copies.append(pltpu.make_async_copy(x_hbm.at[part], x_buf.at[part], x_sem.at[c]))
    w_copies = []
    for j in range(KVH):
        h = head_of((j + 1) % n)
        columns = pl.ds(pl.multiple_of(h * HD, HD), HD)
        for kind, w_hbm in enumerate((wk_hbm, wv_hbm)):
            w_copies.append(pltpu.make_async_copy(
                w_hbm.at[:, columns], weights.at[h, :, pl.ds(kind * HD, HD)], w_sem.at[j, kind]
            ))
    gain_copy = pltpu.make_async_copy(gain_hbm, gain_buf, small_sem.at[0])
    off_copy = pltpu.make_async_copy(off_hbm, off_in, small_sem.at[1])
    q_copy = pltpu.make_async_copy(q_hbm, q_buf, small_sem.at[2])
    bias_copy = pltpu.make_async_copy(bias_hbm, bias_buf, small_sem.at[3])
    gain_copy.start()
    x_copies[0].start()
    w_copies[0].start()
    w_copies[1].start()
    for copy in x_copies[1:]:
        copy.start()
    for copy in w_copies[2:]:
        copy.start()
    off_copy.start()
    q_copy.start()
    bias_copy.start()

    gain_copy.wait()
    gain = gain_buf[...]

    def prepare(c):
        start, count = chunks[c]
        x_copies[c].wait()

        def step(i, _):
            rows = pl.ds(pl.multiple_of(start + i * STEP, STEP), STEP)
            x = x_buf[rows, :].astype(jnp.float32)
            scaled[rows, :] = (x * gain).astype(jnp.bfloat16)
            scale = lax.rsqrt(jnp.mean(x * x, axis=-1, keepdims=True) + EPSILON)
            row_scale[rows, :] = jnp.broadcast_to(scale, (STEP, HD))
            return 0

        lax.fori_loop(0, count // STEP, step, 0, unroll=4)

    def wait_weights(i):
        j = (i - 1) % n
        if j < KVH:
            w_copies[2 * j].wait()
            w_copies[2 * j + 1].wait()

    def project(i, start, count):
        base = lax.div(peer(i), KVH) * block if seqs > 1 else 0
        rows = pl.ds(pl.multiple_of(base + start, STEP) if seqs > 1 else start, count)
        both = jnp.dot(
            scaled[rows, :], weights[head_of(i)], preferred_element_type=jnp.float32
        )
        scale = row_scale[rows, :]
        return [
            (both[:, kind * HD:(kind + 1) * HD] * scale).astype(jnp.bfloat16) for kind in range(2)
        ]

    lands = ((k_land, k_sem), (v_land, v_sem))

    def remote(src, dst, sem, d, target):
        return pltpu.make_async_remote_copy(
            src_ref=src, dst_ref=dst, send_sem=sem.at[0, d], recv_sem=sem.at[1, d],
            device_id={"sp": target}, device_id_type=MESH,
        )

    def block_copy(kind, i, start=0, count=block):
        land, sem = lands[kind]
        there = pl.ds(pl.multiple_of(me * block + start, STEP), count)
        return remote(
            sends.at[kind, i, pl.ds(start, count)], land.at[0, 0, there], sem, offset(i), peer(i)
        )

    def offset_copy(i):
        return remote(off_send.at[peer(i)], off_land.at[me], o_sem, offset(i), peer(i))

    def send(i, start, count):
        for kind, values in enumerate(project(i, start, count)):
            sends[kind, i, pl.ds(start, count)] = values
        if i == 1 and start == 0:
            pl.semaphore_wait(barrier, n - 1)
        for kind in range(2):
            block_copy(kind, i, start, count).start()

    if seqs == 1:
        for c, (start, count) in enumerate(chunks):
            prepare(c)
            if c == 0:
                wait_weights(1)
            send(1, start, count)
    else:
        for c in range(len(chunks)):
            prepare(c)
        wait_weights(1)
        send(1, 0, block)
    off_copy.wait()
    for s in range(seqs):
        values = off_in[s].astype(jnp.float32)
        for h in range(KVH):
            off_send[s * KVH + h] = values[h:h + 1, :]
    off_land[me] = off_send[me]
    for i in order:
        offset_copy(i).start()
    for i in order[1:]:
        wait_weights(i)
        send(i, 0, block)
    wait_weights(0)
    here = pl.ds(pl.multiple_of(me * block, block), block)
    for (land, _), values in zip(lands, project(0, 0, block)):
        land[0, 0, here] = values

    def rows_of(source):
        return pl.ds(pl.multiple_of(source * block, block), block)

    def arrived(kind, source):
        land, sem = lands[kind]
        d = lax.rem(me - source + n, n)
        remote(
            sends.at[kind, 0], land.at[0, 0, rows_of(source)], sem, d, source
        ).wait_recv()

    q_copy.wait()
    q_all = q_buf[0].astype(jnp.float32)
    q_rows = jnp.concatenate([q_all[:, g * HD:(g + 1) * HD] for g in range(GROUP)] * 2, axis=0)
    q_rows = q_rows.astype(jnp.bfloat16)
    bias_copy.wait()
    row_id = lax.broadcasted_iota(jnp.int32, (2 * GROUP, H), 0)
    lane_id = lax.broadcasted_iota(jnp.int32, (2 * GROUP, H), 1)
    chosen = lane_id == lax.rem(me, KVH) * GROUP + lax.rem(row_id, GROUP)
    bias = jnp.sum(jnp.where(chosen, bias_buf[...], 0.0), axis=1, keepdims=True)
    for d in order:
        source = lax.rem(me + n - d, n)
        remote(off_send.at[0], off_land.at[source], o_sem, d, source).wait_recv()
    off_row = jnp.concatenate([off_land[i] for i in range(n)], axis=1)
    off_out[0] = off_row.astype(jnp.bfloat16)

    last = last_source(me, n)

    def source_of(j):
        start = lax.rem(last + 1 + j, n)
        return start

    sources = [source_of(j) for j in range(n - 1)]

    def wait_block(kind, source):
        @pl.when(source != me)
        def _():
            arrived(kind, source)

    for source in sources:
        wait_block(0, source)
    arrived(0, last)
    scores = lax.dot_general(
        q_rows, k_land[0, 0], (((1,), (1,)), ((), ())), preferred_element_type=jnp.float32
    )
    scores = scores / math.sqrt(HD) + bias + off_row
    tail = jnp.log1p(jnp.exp(-jnp.abs(scores)))
    spread = jnp.maximum(scores, 0.0) + tail
    log_sig = jnp.minimum(scores, 0.0) - tail
    pieces = length // HD
    cut = [spread[:, c * HD:(c + 1) * HD] for c in range(pieces)]
    stacked = jnp.concatenate(cut, axis=0)
    after = (
        lax.broadcasted_iota(jnp.int32, (HD, HD), 0) > lax.broadcasted_iota(jnp.int32, (HD, HD), 1)
    ).astype(jnp.float32)
    inner = jnp.dot(
        stacked, after, preferred_element_type=jnp.float32, precision=lax.Precision.HIGHEST
    )
    sums = jnp.sum(stacked, axis=1, keepdims=True)
    carried = jnp.zeros((2 * GROUP, 1), jnp.float32)
    for c in reversed(range(pieces)):
        rows = slice(c * 2 * GROUP, (c + 1) * 2 * GROUP)
        beyond = inner[rows] + carried
        stick[:, c * HD:(c + 1) * HD] = jnp.exp(log_sig[:, c * HD:(c + 1) * HD] - beyond)
        carried = carried + sums[rows]

    mixture = jnp.zeros((2 * GROUP, HD), jnp.float32)
    for source in sources:
        wait_block(1, source)
        part = rows_of(source)
        mixture = mixture + jnp.dot(
            stick[:, part].astype(jnp.bfloat16), v_land[0, 0, part, :],
            preferred_element_type=jnp.float32,
        )
    mix_out[...] = mixture
    for i in order:
        block_copy(0, i).wait_send()
        block_copy(1, i).wait_send()
        offset_copy(i).wait_send()
    arrived(1, last)


def finish(
    n, k_in, v_in, off_in, stick_in, mix_in, k_out, v_out, off_out, read_out, read_buf, sem
):
    copies = [
        pltpu.make_async_copy(src, dst, sem.at[i])
        for i, (src, dst) in enumerate(((k_in, k_out), (v_in, v_out), (off_in, off_out)))
    ]
    for copy in copies:
        copy.start()
    block = v_in.shape[2] // n
    last = last_source(lax.axis_index("sp"), n)
    part = pl.ds(pl.multiple_of(last * block, block), block)
    mixture = mix_in[...] + jnp.dot(
        stick_in[:, part].astype(jnp.bfloat16), v_in[0, 0, part, :],
        preferred_element_type=jnp.float32,
    )
    scale = lax.rsqrt(jnp.mean(mixture * mixture, axis=-1, keepdims=True) + EPSILON)
    read = mixture * scale
    read_buf[0] = jnp.concatenate([read[g:g + 1] for g in range(GROUP)], axis=1).astype(jnp.bfloat16)
    copies.append(pltpu.make_async_copy(read_buf, read_out, sem.at[3]))
    copies[3].start()
    for copy in copies:
        copy.wait()


def chunks_of(seqs, block):
    if seqs > 1:
        return tuple((r, ROWS) for r in range(0, seqs * block, ROWS))
    return ((0, FIRST), (FIRST, ROWS), (FIRST + ROWS, block - FIRST - ROWS))


def shards(layer_input, input_gain, key_weight, value_weight, stick_offsets, head_bias, queries):
    seqs, block, width = layer_input.shape
    n = lax.axis_size("sp")
    length = n * block
    total = seqs * block
    hbm = pl.BlockSpec(memory_space=pltpu.HBM)
    vmem = pl.BlockSpec(memory_space=pltpu.VMEM)
    group_width = queries.shape[-1]
    chunks = chunks_of(seqs, block)
    cache = ((1, 1, length, HD), jnp.bfloat16)
    offsets = ((1, 1, length), jnp.bfloat16)
    read = ((1, 1, group_width), jnp.bfloat16)
    held_outs = (
        cache,
        cache,
        offsets,
        ((2 * GROUP, length), jnp.float32),
        ((2 * GROUP, HD), jnp.float32),
    )
    held = pl.pallas_call(
        functools.partial(kernel, n, seqs, chunks),
        out_shape=tuple(pltpu.VMEM(*out) for out in held_outs),
        in_specs=[hbm] * 7,
        out_specs=(vmem,) * len(held_outs),
        scratch_shapes=[
            pltpu.VMEM((total, width), jnp.bfloat16),
            pltpu.VMEM((total, width), jnp.bfloat16),
            pltpu.VMEM((total, HD), jnp.float32),
            pltpu.VMEM((KVH, width, 2 * HD), jnp.bfloat16),
            pltpu.VMEM((2, n, block, HD), jnp.bfloat16),
            pltpu.VMEM((1, width), jnp.float32),
            pltpu.VMEM((1, H), jnp.float32),
            pltpu.VMEM((seqs, KVH, block), jnp.bfloat16),
            pltpu.VMEM((n, 1, block), jnp.float32),
            pltpu.VMEM((n, 1, block), jnp.float32),
            pltpu.VMEM((1, 1, group_width), jnp.bfloat16),
            pltpu.SemaphoreType.DMA((len(chunks),)),
            pltpu.SemaphoreType.DMA((KVH, 2)),
            pltpu.SemaphoreType.DMA((4,)),
            pltpu.SemaphoreType.DMA((2, n)),
            pltpu.SemaphoreType.DMA((2, n)),
            pltpu.SemaphoreType.DMA((2, n)),
        ],
        compiler_params=pltpu.CompilerParams(
            collective_id=0, has_side_effects=True, vmem_limit_bytes=VMEM_BYTES - 4 * length * HD - SPARE_BYTES
        ),
    )(
        layer_input.reshape(total, width),
        input_gain.reshape(1, width),
        key_weight,
        value_weight,
        jnp.transpose(stick_offsets, (1, 0, 2)),
        head_bias.reshape(1, H),
        queries,
    )
    outs = (cache, cache, offsets, read)
    return pl.pallas_call(
        functools.partial(finish, n),
        out_shape=tuple(jax.ShapeDtypeStruct(*out) for out in outs),
        in_specs=[vmem] * len(held_outs),
        out_specs=(hbm,) * len(outs),
        scratch_shapes=[
            pltpu.VMEM(*read),
            pltpu.SemaphoreType.DMA((len(outs),)),
        ],
        compiler_params=pltpu.CompilerParams(vmem_limit_bytes=WRITE_BYTES),
    )(*held)


def solution(mesh):
    placed = (
        P(("grp", "tp"), "sp", None),
        P(),
        P(),
        P(),
        P(None, ("grp", "tp"), "sp"),
        P(),
        P(("grp", "tp"), "sp", None),
    )
    return jax.shard_map(
        shards,
        mesh=mesh,
        in_specs=placed,
        out_specs=(
            P(("grp", "tp"), "sp", None, None),
            P(("grp", "tp"), "sp", None, None),
            P(("grp", "tp"), "sp", None),
            P(("grp", "tp"), "sp", None),
        ),
        check_vma=False,
    )
```

time: 28.4 us -> 24.1 us (0.85)
  the two profiles are of different devices: /device:TPU:0 before, /device:TPU:8 now
where the time goes in v1:
time: 24.1 us; the launch traced here: 23.9 us
  Pallas kernels  23.3 us (97%)
  between operations  0.64 us (3%)
    pallas_call x1, Pallas kernels, shards(): pl.pallas_call(functools.partial(kernel, n, seqs, chunks), out_shape=tupl...  22.4 us
    pallas_call x1, Pallas kernels, shards(): pl.pallas_call(functools.partial(finish, n), out_shape=tuple((jax.ShapeDt...  0.93 us

profile of v1, /device:TPU:8, one launch (start us, length us, event | category | flops | bytes accessed | tf_op | source)
XLA Modules:
  0.0 23.9 jit_solution(18070831168946597553)
XLA Ops:
  0.6 22.4 %shard_map.102 = (bf16[1,1,1536,128]{3,2,1,0:T(8,128)(2,1)S(1)}, bf16[1,1,1536,128]{3,2,1,0:T(8,128)(2,1)S(1)}, bf16[1,1,1536]{2,1,0:T(2,128)(2,1)S(1)}, f32[8,1536]{1,0:T(8,128)S(1)}, f32[8,128]{1,0:T(8,128)S(1)}) custom-call(bf16[384,2048]{1,0:T(8,128)(2,1)} %bitcast.4, f32[1,2048]{1,0:T(1,128)} %bitcast.5, bf16[2048,512]{1,0:T(8,128)(2,1)} %wk_hbm.1, ...), custom_call_target="tpu_custom_call" | custom-call | tf_op jit(solution)/shard_map/pallas_call | solution.py:307
  23.0 0.9 %shard_map.103 = (bf16[1,1,1536,128]{3,2,1,0:T(8,128)(2,1)}, bf16[1,1,1536,128]{3,2,1,0:T(8,128)(2,1)}, bf16[1,1,1536]{2,1,0:T(2,128)(2,1)}, bf16[1,1,512]{2,1,0:T(2,128)(2,1)}) custom-call(bf16[1,1,1536,128]{3,2,1,0:T(8,128)(2,1)S(1)} %get-tuple-element.9.k_in, bf16[1,1,1536,128]{3,2,1,0:T(8,128)(2,1)S(1)} %get-tuple-element.10.v_in, ...), custom_call_target="tpu_custom_call" | custom-call | tf_op jit(solution)/shard_map/pallas_call | solution.py:344

commit v2 on v1

--- a/solution.py
+++ b/solution.py
@@ -14,7 +14,7 @@
 GROUP = H // KVH
 EPSILON = 1e-06
 ROWS = 128
-FIRST = 64
+FIRST = 128
 STEP = 16
 VMEM_BYTES = 67043328
 SPARE_BYTES = 524288
@@ -30,7 +30,7 @@
     n, seqs, chunks, x_hbm, gain_hbm, wk_hbm, wv_hbm, off_hbm, bias_hbm, q_hbm,
     k_land, v_land, off_out, stick, mix_out,
     x_buf, scaled, row_scale, weights, sends, gain_buf, bias_buf, off_in, off_send, off_land, q_buf,
-    x_sem, w_sem, small_sem, k_sem, v_sem, o_sem,
+    x_sem, w_sem, small_sem, send_sem, k_sem, v_sem, o_sem,
 ):
     total, width = x_buf.shape
     block = total // seqs
@@ -40,20 +40,11 @@
     lower = 2 * me < n
     near = jnp.where(lower, me, n - 1 - me)
 
-    barrier = pltpu.get_barrier_semaphore()
-    for d in order:
-        pl.semaphore_signal(
-            barrier, inc=1, device_id={"sp": lax.rem(me + d, n)}, device_id_type=MESH
-        )
-
     def peer(i):
         if i == 0:
             return me
         far = jnp.where(i <= n - 1 - near, n - i, n - 1 - i)
         return jnp.where(lower, far, n - 1 - far)
-
-    def offset(i):
-        return lax.rem(peer(i) - me + n, n)
 
     def head_of(i):
         return lax.rem(peer(i), KVH)
@@ -64,11 +55,12 @@
         x_copies.append(pltpu.make_async_copy(x_hbm.at[part], x_buf.at[part], x_sem.at[c]))
     w_copies = []
     for j in range(KVH):
-        h = head_of((j + 1) % n)
-        columns = pl.ds(pl.multiple_of(h * HD, HD), HD)
+        columns = pl.ds(pl.multiple_of(head_of((j + 1) % n) * HD, HD), HD)
         for kind, w_hbm in enumerate((wk_hbm, wv_hbm)):
             w_copies.append(pltpu.make_async_copy(
-                w_hbm.at[:, columns], weights.at[h, :, pl.ds(kind * HD, HD)], w_sem.at[j, kind]
+                w_hbm.at[:, columns],
+                weights.at[j, :, pl.ds(kind * HD, HD)],
+                w_sem.at[min(j, 1)],
             ))
     gain_copy = pltpu.make_async_copy(gain_hbm, gain_buf, small_sem.at[0])
     off_copy = pltpu.make_async_copy(off_hbm, off_in, small_sem.at[1])
@@ -80,11 +72,11 @@
     w_copies[1].start()
     for copy in x_copies[1:]:
         copy.start()
-    for copy in w_copies[2:]:
-        copy.start()
-    off_copy.start()
-    q_copy.start()
-    bias_copy.start()
+    barrier = pltpu.get_barrier_semaphore()
+    for d in order:
+        pl.semaphore_signal(
+            barrier, inc=1, device_id={"sp": lax.rem(me + d, n)}, device_id_type=MESH
+        )
 
     gain_copy.wait()
     gain = gain_buf[...]
@@ -104,43 +96,65 @@
         lax.fori_loop(0, count // STEP, step, 0, unroll=4)
 
     def wait_weights(i):
-        j = (i - 1) % n
-        if j < KVH:
-            w_copies[2 * j].wait()
-            w_copies[2 * j + 1].wait()
+        if i == 1:
+            part = weights.at[pl.ds(0, 1)]
+            pltpu.make_async_copy(part, part, w_sem.at[0]).wait()
+            for copy in w_copies[2:]:
+                copy.start()
+            off_copy.start()
+            q_copy.start()
+            bias_copy.start()
+        if i == 2 % n:
+            part = weights.at[pl.ds(1, KVH - 1)]
+            pltpu.make_async_copy(part, part, w_sem.at[1]).wait()
+
+    def slot(i):
+        if n == KVH:
+            return (i - 1) % n
+        first = head_of(1)
+        down = lax.rem(first - head_of(i) + KVH, KVH)
+        return jnp.where(lower, down, lax.rem(KVH - down, KVH))
 
     def project(i, start, count):
         base = lax.div(peer(i), KVH) * block if seqs > 1 else 0
         rows = pl.ds(pl.multiple_of(base + start, STEP) if seqs > 1 else start, count)
         both = jnp.dot(
-            scaled[rows, :], weights[head_of(i)], preferred_element_type=jnp.float32
+            scaled[rows, :], weights[slot(i)], preferred_element_type=jnp.float32
         )
         scale = row_scale[rows, :]
         return [
             (both[:, kind * HD:(kind + 1) * HD] * scale).astype(jnp.bfloat16) for kind in range(2)
         ]
 
-    lands = ((k_land, k_sem), (v_land, v_sem))
-
-    def remote(src, dst, sem, d, target):
+    lands = (k_land, v_land)
+
+    def remote(src, dst, sent, landed, target):
         return pltpu.make_async_remote_copy(
-            src_ref=src, dst_ref=dst, send_sem=sem.at[0, d], recv_sem=sem.at[1, d],
+            src_ref=src, dst_ref=dst, send_sem=send_sem.at[sent], recv_sem=landed,
             device_id={"sp": target}, device_id_type=MESH,
         )
 
-    def block_copy(kind, i, start=0, count=block):
-        land, sem = lands[kind]
+    def landed_sem(kind, source, target):
+        if kind == 0:
+            return k_sem.at[0]
+        return v_sem.at[jnp.where(source == last_source(target, n), 1, 0)]
+
+    def block_copy(kind, i, start, count):
         there = pl.ds(pl.multiple_of(me * block + start, STEP), count)
         return remote(
-            sends.at[kind, i, pl.ds(start, count)], land.at[0, 0, there], sem, offset(i), peer(i)
+            sends.at[i - 1, kind, pl.ds(start, count)],
+            lands[kind].at[0, 0, there],
+            0,
+            landed_sem(kind, me, peer(i)),
+            peer(i),
         )
 
     def offset_copy(i):
-        return remote(off_send.at[peer(i)], off_land.at[me], o_sem, offset(i), peer(i))
+        return remote(off_send.at[peer(i)], off_land.at[me], 1, o_sem.at[0], peer(i))
 
     def send(i, start, count):
         for kind, values in enumerate(project(i, start, count)):
-            sends[kind, i, pl.ds(start, count)] = values
+            sends[i - 1, kind, pl.ds(start, count)] = values
         if i == 1 and start == 0:
             pl.semaphore_wait(barrier, n - 1)
         for kind in range(2):
@@ -170,18 +184,15 @@
         send(i, 0, block)
     wait_weights(0)
     here = pl.ds(pl.multiple_of(me * block, block), block)
-    for (land, _), values in zip(lands, project(0, 0, block)):
+    for land, values in zip(lands, project(0, 0, block)):
         land[0, 0, here] = values
 
     def rows_of(source):
         return pl.ds(pl.multiple_of(source * block, block), block)
 
-    def arrived(kind, source):
-        land, sem = lands[kind]
-        d = lax.rem(me - source + n, n)
-        remote(
-            sends.at[kind, 0], land.at[0, 0, rows_of(source)], sem, d, source
-        ).wait_recv()
+    def arrived(kind, blocks, sem):
+        part = lands[kind].at[0, 0, pl.ds(0, blocks * block)]
+        remote(part, part, 0, sem, peer(1)).wait_recv()
 
     q_copy.wait()
     q_all = q_buf[0].astype(jnp.float32)
@@ -192,28 +203,14 @@
     lane_id = lax.broadcasted_iota(jnp.int32, (2 * GROUP, H), 1)
     chosen = lane_id == lax.rem(me, KVH) * GROUP + lax.rem(row_id, GROUP)
     bias = jnp.sum(jnp.where(chosen, bias_buf[...], 0.0), axis=1, keepdims=True)
-    for d in order:
-        source = lax.rem(me + n - d, n)
-        remote(off_send.at[0], off_land.at[source], o_sem, d, source).wait_recv()
+    part = off_land.at[pl.ds(0, n - 1)]
+    remote(part, part, 1, o_sem.at[0], peer(1)).wait_recv()
     off_row = jnp.concatenate([off_land[i] for i in range(n)], axis=1)
     off_out[0] = off_row.astype(jnp.bfloat16)
 
     last = last_source(me, n)
 
-    def source_of(j):
-        start = lax.rem(last + 1 + j, n)
-        return start
-
-    sources = [source_of(j) for j in range(n - 1)]
-
-    def wait_block(kind, source):
-        @pl.when(source != me)
-        def _():
-            arrived(kind, source)
-
-    for source in sources:
-        wait_block(0, source)
-    arrived(0, last)
+    arrived(0, n - 1, k_sem.at[0])
     scores = lax.dot_general(
         q_rows, k_land[0, 0], (((1,), (1,)), ((), ())), preferred_element_type=jnp.float32
     )
@@ -238,20 +235,20 @@
         stick[:, c * HD:(c + 1) * HD] = jnp.exp(log_sig[:, c * HD:(c + 1) * HD] - beyond)
         carried = carried + sums[rows]
 
+    if n > 2:
+        arrived(1, n - 2, v_sem.at[0])
     mixture = jnp.zeros((2 * GROUP, HD), jnp.float32)
-    for source in sources:
-        wait_block(1, source)
-        part = rows_of(source)
+    for j in range(n - 1):
+        part = rows_of(lax.rem(last + 1 + j, n))
         mixture = mixture + jnp.dot(
             stick[:, part].astype(jnp.bfloat16), v_land[0, 0, part, :],
             preferred_element_type=jnp.float32,
         )
     mix_out[...] = mixture
-    for i in order:
-        block_copy(0, i).wait_send()
-        block_copy(1, i).wait_send()
-        offset_copy(i).wait_send()
-    arrived(1, last)
+    remote(sends, sends, 0, k_sem.at[0], peer(1)).wait_send()
+    part = off_send.at[pl.ds(0, n - 1)]
+    remote(part, part, 1, o_sem.at[0], peer(1)).wait_send()
+    arrived(1, 1, v_sem.at[1])
 
 
 def finish(
@@ -282,7 +279,7 @@
 def chunks_of(seqs, block):
     if seqs > 1:
         return tuple((r, ROWS) for r in range(0, seqs * block, ROWS))
-    return ((0, FIRST), (FIRST, ROWS), (FIRST + ROWS, block - FIRST - ROWS))
+    return ((0, FIRST), (FIRST, block - FIRST))
 
 
 def shards(layer_input, input_gain, key_weight, value_weight, stick_offsets, head_bias, queries):
@@ -314,7 +311,7 @@
             pltpu.VMEM((total, width), jnp.bfloat16),
             pltpu.VMEM((total, HD), jnp.float32),
             pltpu.VMEM((KVH, width, 2 * HD), jnp.bfloat16),
-            pltpu.VMEM((2, n, block, HD), jnp.bfloat16),
+            pltpu.VMEM((n - 1, 2, block, HD), jnp.bfloat16),
             pltpu.VMEM((1, width), jnp.float32),
             pltpu.VMEM((1, H), jnp.float32),
             pltpu.VMEM((seqs, KVH, block), jnp.bfloat16),
@@ -322,11 +319,12 @@
             pltpu.VMEM((n, 1, block), jnp.float32),
             pltpu.VMEM((1, 1, group_width), jnp.bfloat16),
             pltpu.SemaphoreType.DMA((len(chunks),)),
-            pltpu.SemaphoreType.DMA((KVH, 2)),
+            pltpu.SemaphoreType.DMA((2,)),
             pltpu.SemaphoreType.DMA((4,)),
-            pltpu.SemaphoreType.DMA((2, n)),
-            pltpu.SemaphoreType.DMA((2, n)),
-            pltpu.SemaphoreType.DMA((2, n)),
+            pltpu.SemaphoreType.DMA((2,)),
+            pltpu.SemaphoreType.DMA((1,)),
+            pltpu.SemaphoreType.DMA((2,)),
+            pltpu.SemaphoreType.DMA((1,)),
         ],
         compiler_params=pltpu.CompilerParams(
             collective_id=0, has_side_effects=True, vmem_limit_bytes=VMEM_BYTES - 4 * length * HD - SPARE_BYTES

time: 24.1 us -> 23.1 us (0.959)
  Pallas kernels: 23.3 us -> 22.3 us
    pallas_call x1, Pallas kernels: 22.4 us -> 21.4 us  [shards(): pl.pallas_call(functools.partial(kernel, n, seqs, chunks), out_shape=tupl...]
where the time goes in v2:
time: 23.1 us; the launch traced here: 23 us
  Pallas kernels  22.3 us (97%)
  between operations  0.64 us (3%)
    pallas_call x1, Pallas kernels, shards(): pl.pallas_call(functools.partial(kernel, n, seqs, chunks), out_shape=tupl...  21.4 us
    pallas_call x1, Pallas kernels, shards(): pl.pallas_call(functools.partial(finish, n), out_shape=tuple((jax.ShapeDt...  0.93 us

profile of v2, /device:TPU:8, one launch (start us, length us, event | category | flops | bytes accessed | tf_op | source)
XLA Modules:
  0.0 23.0 jit_solution(17232504113543955431)
XLA Ops:
  0.6 21.4 %shard_map.102 = (bf16[1,1,1536,128]{3,2,1,0:T(8,128)(2,1)S(1)}, bf16[1,1,1536,128]{3,2,1,0:T(8,128)(2,1)S(1)}, bf16[1,1,1536]{2,1,0:T(2,128)(2,1)S(1)}, f32[8,1536]{1,0:T(8,128)S(1)}, f32[8,128]{1,0:T(8,128)S(1)}) custom-call(bf16[384,2048]{1,0:T(8,128)(2,1)} %bitcast.4, f32[1,2048]{1,0:T(1,128)} %bitcast.5, bf16[2048,512]{1,0:T(8,128)(2,1)} %wk_hbm.1, ...), custom_call_target="tpu_custom_call" | custom-call | tf_op jit(solution)/shard_map/pallas_call | solution.py:304
  22.1 0.9 %shard_map.103 = (bf16[1,1,1536,128]{3,2,1,0:T(8,128)(2,1)}, bf16[1,1,1536,128]{3,2,1,0:T(8,128)(2,1)}, bf16[1,1,1536]{2,1,0:T(2,128)(2,1)}, bf16[1,1,512]{2,1,0:T(2,128)(2,1)}) custom-call(bf16[1,1,1536,128]{3,2,1,0:T(8,128)(2,1)S(1)} %get-tuple-element.9.k_in, bf16[1,1,1536,128]{3,2,1,0:T(8,128)(2,1)S(1)} %get-tuple-element.10.v_in, ...), custom_call_target="tpu_custom_call" | custom-call | tf_op jit(solution)/shard_map/pallas_call | solution.py:342

commit v3 on v2

v3 whole, which is shorter than its diff:
```python
import functools
import math

import jax
import jax.numpy as jnp
from jax import lax
from jax.experimental import pallas as pl
from jax.experimental.pallas import tpu as pltpu
from jax.sharding import PartitionSpec as P

H = 16
KVH = 4
HD = 128
GROUP = H // KVH
EPSILON = 1e-06
ROWS = 128
STEP = 16
TILE = 8
DEPTH = 256
VMEM_BYTES = 67043328
SPARE_BYTES = 524288
WRITE_BYTES = 1048576
MESH = pl.DeviceIdType.MESH


def last_source(me, n):
    return jnp.where(2 * me < n, n // 2, n // 2 - 1)


def unit_rows(block):
    return 2 * block + -(-block // (HD * TILE)) * TILE


def kernel(
    n, seqs, chunks, x_hbm, gain_hbm, wk_hbm, wv_hbm, off_hbm, bias_hbm, q_hbm,
    land, off_out, stick, mix_out,
    x_buf, scaled, row_scale, weights, sends, gain_buf, bias_buf, off_in, off_tiles, q_buf,
    x_sem, w_sem, small_sem, land_sem,
):
    total, width = x_buf.shape
    block = total // seqs
    length = n * block
    unit = unit_rows(block)
    me = lax.axis_index("sp")
    order = range(1, n)
    lower = 2 * me < n
    near = jnp.where(lower, me, n - 1 - me)

    def peer(i):
        if i == 0:
            return me
        far = jnp.where(i <= n - 1 - near, n - i, n - 1 - i)
        return jnp.where(lower, far, n - 1 - far)

    def head_of(i):
        return lax.rem(peer(i), KVH)

    gain_copy = pltpu.make_async_copy(gain_hbm, gain_buf, small_sem.at[0])
    x_copies = []
    for c, (start, rows) in enumerate(chunks):
        part = pl.ds(start, rows)
        x_copies.append(pltpu.make_async_copy(x_hbm.at[part], x_buf.at[part], x_sem.at[c]))
    w_copies = []
    for j in range(KVH):
        columns = pl.ds(pl.multiple_of(head_of((j + 1) % n) * HD, HD), HD)
        for kind, w_hbm in enumerate((wk_hbm, wv_hbm)):
            w_copies.append(pltpu.make_async_copy(
                w_hbm.at[:, columns],
                weights.at[j, :, pl.ds(kind * HD, HD)],
                w_sem.at[0 if j else kind],
            ))
    off_copy = pltpu.make_async_copy(off_hbm, off_in, small_sem.at[1])
    q_copy = pltpu.make_async_copy(q_hbm, q_buf, small_sem.at[0])
    bias_copy = pltpu.make_async_copy(bias_hbm, bias_buf, x_sem.at[1])
    gain_copy.start()
    x_copies[0].start()
    w_copies[0].start()
    w_copies[1].start()
    for copy in x_copies[1:]:
        copy.start()
    off_copy.start()

    barrier = pltpu.get_barrier_semaphore()
    for d in order:
        pl.semaphore_signal(
            barrier, inc=1, device_id={"sp": lax.rem(me + d, n)}, device_id_type=MESH
        )

    gain_copy.wait()
    gain = gain_buf[...]

    def prepare(c):
        start, count = chunks[c]
        x_copies[c].wait()

        def step(i, _):
            rows = pl.ds(pl.multiple_of(start + i * STEP, STEP), STEP)
            x = x_buf[rows, :].astype(jnp.float32)
            scaled[rows, :] = (x * gain).astype(jnp.bfloat16)
            scale = lax.rsqrt(jnp.mean(x * x, axis=-1, keepdims=True) + EPSILON)
            row_scale[rows, :] = jnp.broadcast_to(scale, (STEP, HD))
            return 0

        lax.fori_loop(0, count // STEP, step, 0, unroll=4)

    def later_loads():
        for copy in w_copies[2:]:
            copy.start()
        q_copy.start()

    def wait_weights(i):
        if i == 2 % n:
            part = weights.at[pl.ds(1, KVH - 1)]
            pltpu.make_async_copy(part, part, w_sem.at[0]).wait()

    def slot(i):
        if n == KVH:
            return (i - 1) % n
        first = head_of(1)
        down = lax.rem(first - head_of(i) + KVH, KVH)
        return jnp.where(lower, down, lax.rem(KVH - down, KVH))

    def project(i, start, count, columns):
        base = lax.div(peer(i), KVH) * block if seqs > 1 else 0
        rows = pl.ds(pl.multiple_of(base + start, STEP) if seqs > 1 else start, count)
        product = jnp.dot(
            scaled[rows, :], weights[slot(i), :, columns], preferred_element_type=jnp.float32
        )
        scale = row_scale[rows, :]
        return [
            (product[:, c:c + HD] * scale).astype(jnp.bfloat16)
            for c in range(0, product.shape[1], HD)
        ]

    def prepare_and_project(start, count, columns):
        rows = pl.ds(start, count)
        product = jnp.zeros((count, columns.size), jnp.float32)
        squares = jnp.zeros((count, HD), jnp.float32)
        for k in range(0, width, DEPTH):
            part = pl.ds(k, DEPTH)
            x = x_buf[rows, part].astype(jnp.float32)
            y = (x * gain[:, k:k + DEPTH]).astype(jnp.bfloat16)
            scaled[rows, part] = y
            for c in range(0, DEPTH, HD):
                squares = squares + x[:, c:c + HD] * x[:, c:c + HD]
            product = product + jnp.dot(
                y, weights[slot(1), part, columns], preferred_element_type=jnp.float32
            )
        scale = lax.rsqrt(jnp.sum(squares, axis=-1, keepdims=True) / width + EPSILON)
        scale = jnp.broadcast_to(scale, (count, HD))
        row_scale[rows, :] = scale
        return [
            (product[:, c:c + HD] * scale).astype(jnp.bfloat16)
            for c in range(0, columns.size, HD)
        ]

    def remote(src, dst, landed, target):
        return pltpu.make_async_remote_copy(
            src_ref=src, dst_ref=dst, send_sem=x_sem.at[0], recv_sem=landed,
            device_id={"sp": target}, device_id_type=MESH,
        )

    key_part, value_part = pl.ds(0, block), pl.ds(block, block)
    off_part = pl.ds(2 * block, unit - 2 * block)

    def copy_out(i, part, is_value=False):
        is_last = me == last_source(peer(i), n)
        sem = land_sem.at[jnp.where(is_last, 2 if is_value else 1, 0)]
        remote(sends.at[i - 1, part], land.at[me, part], sem, peer(i)).start()

    def lay_offsets():
        off_copy.wait()
        for s in range(seqs):
            values = off_in[s].astype(jnp.float32)
            for h in range(KVH):
                rows = [values[h:h + 1, c:c + HD] for c in range(0, block, HD)]
                blank = jnp.zeros((unit - 2 * block - len(rows), HD), jnp.float32)
                tile = jnp.concatenate(rows + [blank], axis=0)
                off_tiles[s * KVH + h] = tile.astype(jnp.bfloat16)
        for i in order:
            sends[i - 1, off_part] = off_tiles[peer(i)]
        land[me, off_part] = off_tiles[me]

    def greet():
        pl.semaphore_wait(barrier, n - 1)
        for i in order:
            copy_out(i, off_part)

    both = pl.ds(0, 2 * HD)
    lay_offsets()
    if seqs == 1:
        for c, (start, count) in enumerate(chunks):
            x_copies[c].wait()
            keys, values = pl.ds(start, count), pl.ds(block + start, count)
            if c == 0:
                greet()
                w_copies[0].wait()
                sends[0, keys], = prepare_and_project(start, count, pl.ds(0, HD))
                copy_out(1, keys)
                w_copies[1].wait()
                later_loads()
                sends[0, values], = project(1, start, count, pl.ds(HD, HD))
            else:
                sends[0, keys], sends[0, values] = prepare_and_project(start, count, both)
                copy_out(1, keys)
            copy_out(1, values, True)
    else:
        for c in range(len(chunks)):
            prepare(c)
        w_copies[0].wait()
        w_copies[1].wait()
        later_loads()
        sends[0, key_part], sends[0, value_part] = project(1, 0, block, both)
        greet()
        copy_out(1, key_part)
        copy_out(1, value_part, True)
    bias_copy.start()
    for i in order[1:]:
        wait_weights(i)
        sends[i - 1, key_part], sends[i - 1, value_part] = project(i, 0, block, both)
        if i > n // 2:
            copy_out(i, pl.ds(0, 2 * block))
        else:
            copy_out(i, key_part)
            copy_out(i, value_part, True)
    wait_weights(0)
    land[me, key_part], land[me, value_part] = project(0, 0, block, both)

    q_copy.wait()
    q_all = q_buf[0].astype(jnp.float32)
    q_rows = jnp.concatenate([q_all[:, g * HD:(g + 1) * HD] for g in range(GROUP)] * 2, axis=0)
    q_rows = q_rows.astype(jnp.bfloat16)
    bias_copy.wait()
    row_id = lax.broadcasted_iota(jnp.int32, (2 * GROUP, H), 0)
    lane_id = lax.broadcasted_iota(jnp.int32, (2 * GROUP, H), 1)
    chosen = lane_id == lax.rem(me, KVH) * GROUP + lax.rem(row_id, GROUP)
    bias = jnp.sum(jnp.where(chosen, bias_buf[...], 0.0), axis=1, keepdims=True)

    def arrived(part, sem):
        remote(part, part, sem, peer(1)).wait_recv()

    if n > 2:
        arrived(land.at[pl.ds(0, n - 2)], land_sem.at[0])
    arrived(land.at[0, pl.ds(block, unit - block)], land_sem.at[1])
    off_rows = []
    scores = []
    for source in range(n):
        tile = land[source, off_part].astype(jnp.float32)
        off_rows += [tile[c:c + 1] for c in range(block // HD)]
        scores.append(lax.dot_general(
            q_rows, land[source, key_part], (((1,), (1,)), ((), ())),
            preferred_element_type=jnp.float32,
        ))
    off_row = jnp.concatenate(off_rows, axis=1)
    off_out[0] = off_row.astype(jnp.bfloat16)
    scores = jnp.concatenate(scores, axis=1) / math.sqrt(HD) + bias + off_row
    tail = jnp.log1p(jnp.exp(-jnp.abs(scores)))
    spread = jnp.maximum(scores, 0.0) + tail
    log_sig = jnp.minimum(scores, 0.0) - tail
    pieces = length // HD
    cut = [spread[:, c * HD:(c + 1) * HD] for c in range(pieces)]
    stacked = jnp.concatenate(cut, axis=0)
    after = (
        lax.broadcasted_iota(jnp.int32, (HD, HD), 0) > lax.broadcasted_iota(jnp.int32, (HD, HD), 1)
    ).astype(jnp.float32)
    inner = jnp.dot(
        stacked, after, preferred_element_type=jnp.float32, precision=lax.Precision.HIGHEST
    )
    sums = jnp.sum(stacked, axis=1, keepdims=True)
    carried = jnp.zeros((2 * GROUP, 1), jnp.float32)
    for c in reversed(range(pieces)):
        rows = slice(c * 2 * GROUP, (c + 1) * 2 * GROUP)
        beyond = inner[rows] + carried
        stick[:, c * HD:(c + 1) * HD] = jnp.exp(log_sig[:, c * HD:(c + 1) * HD] - beyond)
        carried = carried + sums[rows]

    mixture = jnp.zeros((2 * GROUP, HD), jnp.float32)
    for j in range(n - 1):
        source = lax.rem(last_source(me, n) + 1 + j, n)
        mixture = mixture + read_block(stick, land, source, block)
    mix_out[...] = mixture
    remote(sends, sends, land_sem.at[0], peer(1)).wait_send()
    arrived(land.at[0, value_part], land_sem.at[2])


def read_block(stick, land, source, block):
    part = pl.ds(pl.multiple_of(source * block, block), block)
    return jnp.dot(
        stick[:, part].astype(jnp.bfloat16), land[source, pl.ds(block, block)],
        preferred_element_type=jnp.float32,
    )


def finish(n, land, off_in, stick, mix_in, k_out, v_out, off_out, read_out, read_buf, sem):
    block = k_out.shape[2] // n
    for source in range(n):
        there = pl.ds(source * block, block)
        for kind, cache in enumerate((k_out, v_out)):
            pltpu.make_async_copy(
                land.at[source, pl.ds(kind * block, block)], cache.at[0, 0, there], sem.at[kind]
            ).start()
    off_copy = pltpu.make_async_copy(off_in, off_out, sem.at[2])
    off_copy.start()
    mixture = mix_in[...] + read_block(stick, land, last_source(lax.axis_index("sp"), n), block)
    scale = lax.rsqrt(jnp.mean(mixture * mixture, axis=-1, keepdims=True) + EPSILON)
    read = mixture * scale
    read_buf[0] = jnp.concatenate([read[g:g + 1] for g in range(GROUP)], axis=1).astype(jnp.bfloat16)
    read_copy = pltpu.make_async_copy(read_buf, read_out, sem.at[3])
    read_copy.start()
    for kind, cache in enumerate((k_out, v_out)):
        pltpu.make_async_copy(cache, cache, sem.at[kind]).wait()
    off_copy.wait()
    read_copy.wait()


def chunks_of(seqs, block):
    return tuple((r, ROWS) for r in range(0, seqs * block, ROWS))


def shards(layer_input, input_gain, key_weight, value_weight, stick_offsets, head_bias, queries):
    seqs, block, width = layer_input.shape
    n = lax.axis_size("sp")
    length = n * block
    total = seqs * block
    unit = unit_rows(block)
    hbm = pl.BlockSpec(memory_space=pltpu.HBM)
    vmem = pl.BlockSpec(memory_space=pltpu.VMEM)
    group_width = queries.shape[-1]
    chunks = chunks_of(seqs, block)
    cache = ((1, 1, length, HD), jnp.bfloat16)
    offsets = ((1, 1, length), jnp.bfloat16)
    read = ((1, 1, group_width), jnp.bfloat16)
    held_outs = (
        ((n, unit, HD), jnp.bfloat16),
        offsets,
        ((2 * GROUP, length), jnp.float32),
        ((2 * GROUP, HD), jnp.float32),
    )
    held = pl.pallas_call(
        functools.partial(kernel, n, seqs, chunks),
        out_shape=tuple(pltpu.VMEM(*out) for out in held_outs),
        in_specs=[hbm] * 7,
        out_specs=(vmem,) * len(held_outs),
        scratch_shapes=[
            pltpu.VMEM((total, width), jnp.bfloat16),
            pltpu.VMEM((total, width), jnp.bfloat16),
            pltpu.VMEM((total, HD), jnp.float32),
            pltpu.VMEM((KVH, width, 2 * HD), jnp.bfloat16),
            pltpu.VMEM((n - 1, unit, HD), jnp.bfloat16),
            pltpu.VMEM((1, width), jnp.float32),
            pltpu.VMEM((1, H), jnp.float32),
            pltpu.VMEM((seqs, KVH, block), jnp.bfloat16),
            pltpu.VMEM((n, unit - 2 * block, HD), jnp.bfloat16),
            pltpu.VMEM((1, 1, group_width), jnp.bfloat16),
            pltpu.SemaphoreType.DMA((len(chunks),)),
            pltpu.SemaphoreType.DMA((2,)),
            pltpu.SemaphoreType.DMA((2,)),
            pltpu.SemaphoreType.DMA((3,)),
        ],
        compiler_params=pltpu.CompilerParams(
            collective_id=0, has_side_effects=True, vmem_limit_bytes=VMEM_BYTES - 4 * length * HD - SPARE_BYTES
        ),
    )(
        layer_input.reshape(total, width),
        input_gain.reshape(1, width),
        key_weight,
        value_weight,
        jnp.transpose(stick_offsets, (1, 0, 2)),
        head_bias.reshape(1, H),
        queries,
    )
    outs = (cache, cache, offsets, read)
    return pl.pallas_call(
        functools.partial(finish, n),
        out_shape=tuple(jax.ShapeDtypeStruct(*out) for out in outs),
        in_specs=[vmem] * len(held_outs),
        out_specs=(hbm,) * len(outs),
        scratch_shapes=[
            pltpu.VMEM(*read),
            pltpu.SemaphoreType.DMA((len(outs),)),
        ],
        compiler_params=pltpu.CompilerParams(vmem_limit_bytes=WRITE_BYTES),
    )(*held)


def solution(mesh):
    placed = (
        P(("grp", "tp"), "sp", None),
        P(),
        P(),
        P(),
        P(None, ("grp", "tp"), "sp"),
        P(),
        P(("grp", "tp"), "sp", None),
    )
    return jax.shard_map(
        shards,
        mesh=mesh,
        in_specs=placed,
        out_specs=(
            P(("grp", "tp"), "sp", None, None),
            P(("grp", "tp"), "sp", None, None),
            P(("grp", "tp"), "sp", None),
            P(("grp", "tp"), "sp", None),
        ),
        check_vma=False,
    )
```

time: 23.1 us -> 23 us (level)
  no operation moved by 1% of the time
where the time goes in v3:
time: 23 us; the launch traced here: 22.8 us
  Pallas kernels  22.2 us (97%)
  between operations  0.64 us (3%)
    pallas_call x1, Pallas kernels, shards(): pl.pallas_call(functools.partial(kernel, n, seqs, chunks), out_shape=tupl...  21.2 us
    pallas_call x1, Pallas kernels, shards(): pl.pallas_call(functools.partial(finish, n), out_shape=tuple((jax.ShapeDt...  0.92 us

profile of v3, /device:TPU:8, one launch (start us, length us, event | category | flops | bytes accessed | tf_op | source)
XLA Modules:
  0.0 22.8 jit_solution(15289253916361492337)
XLA Ops:
  0.6 21.2 %shard_map.102 = (bf16[4,776,128]{2,1,0:T(8,128)(2,1)S(1)}, bf16[1,1,1536]{2,1,0:T(2,128)(2,1)S(1)}, f32[8,1536]{1,0:T(8,128)S(1)}, f32[8,128]{1,0:T(8,128)S(1)}) custom-call(bf16[384,2048]{1,0:T(8,128)(2,1)} %bitcast.4, f32[1,2048]{1,0:T(1,128)} %bitcast.5, bf16[2048,512]{1,0:T(8,128)(2,1)} %wk_hbm.1, bf16[2048,512]{1,0:T(8,128)(2,1)} %wv_hbm.1, ...), custom_call_target="tpu_custom_call" | custom-call | tf_op jit(solution)/shard_map/pallas_call | solution.py:339
  21.9 0.9 %shard_map.103 = (bf16[1,1,1536,128]{3,2,1,0:T(8,128)(2,1)}, bf16[1,1,1536,128]{3,2,1,0:T(8,128)(2,1)}, bf16[1,1,1536]{2,1,0:T(2,128)(2,1)}, bf16[1,1,512]{2,1,0:T(2,128)(2,1)}) custom-call(bf16[4,776,128]{2,1,0:T(8,128)(2,1)S(1)} %get-tuple-element.8.land, bf16[1,1,1536]{2,1,0:T(2,128)(2,1)S(1)} %get-tuple-element.9.off_in, ...), custom_call_target="tpu_custom_call" | custom-call | tf_op jit(solution)/shard_map/pallas_call | solution.py:373

commit v4 on v3

--- a/solution.py
+++ b/solution.py
@@ -49,6 +49,8 @@
     def peer(i):
         if i == 0:
             return me
+        if i == 1:
+            return jnp.where(lower, n - 1, 0)
         far = jnp.where(i <= n - 1 - near, n - i, n - 1 - i)
         return jnp.where(lower, far, n - 1 - far)
 
@@ -187,18 +189,23 @@
             copy_out(i, off_part)
 
     both = pl.ds(0, 2 * HD)
-    lay_offsets()
+    if seqs > 1:
+        lay_offsets()
     if seqs == 1:
         for c, (start, count) in enumerate(chunks):
             x_copies[c].wait()
+            if c == len(chunks) - 1:
+                later_loads()
             keys, values = pl.ds(start, count), pl.ds(block + start, count)
             if c == 0:
-                greet()
                 w_copies[0].wait()
                 sends[0, keys], = prepare_and_project(start, count, pl.ds(0, HD))
+                pl.semaphore_wait(barrier, n - 1)
                 copy_out(1, keys)
+                lay_offsets()
+                for i in order:
+                    copy_out(i, off_part)
                 w_copies[1].wait()
-                later_loads()
                 sends[0, values], = project(1, start, count, pl.ds(HD, HD))
             else:
                 sends[0, keys], sends[0, values] = prepare_and_project(start, count, both)

time: 23 us -> 22.6 us (0.983)
  Pallas kernels: 22.2 us -> 21.8 us
    pallas_call x1, Pallas kernels: 21.2 us -> 20.9 us  [shards(): pl.pallas_call(functools.partial(kernel, n, seqs, chunks), out_shape=tupl...]
where the time goes in v4:
time: 22.6 us; the launch traced here: 22.5 us
  Pallas kernels  21.8 us (96%)
  between operations  0.64 us (3%)
    pallas_call x1, Pallas kernels, shards(): pl.pallas_call(functools.partial(kernel, n, seqs, chunks), out_shape=tupl...  20.9 us
    pallas_call x1, Pallas kernels, shards(): pl.pallas_call(functools.partial(finish, n), out_shape=tuple((jax.ShapeDt...  0.92 us

profile of v4, /device:TPU:8, one launch (start us, length us, event | category | flops | bytes accessed | tf_op | source)
XLA Modules:
  0.0 22.5 jit_solution(11918222968879551460)
XLA Ops:
  0.6 20.9 %shard_map.102 = (bf16[4,776,128]{2,1,0:T(8,128)(2,1)S(1)}, bf16[1,1,1536]{2,1,0:T(2,128)(2,1)S(1)}, f32[8,1536]{1,0:T(8,128)S(1)}, f32[8,128]{1,0:T(8,128)S(1)}) custom-call(bf16[384,2048]{1,0:T(8,128)(2,1)} %bitcast.4, f32[1,2048]{1,0:T(1,128)} %bitcast.5, bf16[2048,512]{1,0:T(8,128)(2,1)} %wk_hbm.1, bf16[2048,512]{1,0:T(8,128)(2,1)} %wv_hbm.1, ...), custom_call_target="tpu_custom_call" | custom-call | tf_op jit(solution)/shard_map/pallas_call | solution.py:346
  21.6 0.9 %shard_map.103 = (bf16[1,1,1536,128]{3,2,1,0:T(8,128)(2,1)}, bf16[1,1,1536,128]{3,2,1,0:T(8,128)(2,1)}, bf16[1,1,1536]{2,1,0:T(2,128)(2,1)}, bf16[1,1,512]{2,1,0:T(2,128)(2,1)}) custom-call(bf16[4,776,128]{2,1,0:T(8,128)(2,1)S(1)} %get-tuple-element.8.land, bf16[1,1,1536]{2,1,0:T(2,128)(2,1)S(1)} %get-tuple-element.9.off_in, ...), custom_call_target="tpu_custom_call" | custom-call | tf_op jit(solution)/shard_map/pallas_call | solution.py:380

commit v5 on v4

--- a/solution.py
+++ b/solution.py
@@ -304,18 +304,18 @@
         there = pl.ds(source * block, block)
         for kind, cache in enumerate((k_out, v_out)):
             pltpu.make_async_copy(
-                land.at[source, pl.ds(kind * block, block)], cache.at[0, 0, there], sem.at[kind]
+                land.at[source, pl.ds(kind * block, block)], cache.at[0, 0, there], sem.at[0]
             ).start()
-    off_copy = pltpu.make_async_copy(off_in, off_out, sem.at[2])
+    off_copy = pltpu.make_async_copy(off_in, off_out, sem.at[1])
     off_copy.start()
     mixture = mix_in[...] + read_block(stick, land, last_source(lax.axis_index("sp"), n), block)
     scale = lax.rsqrt(jnp.mean(mixture * mixture, axis=-1, keepdims=True) + EPSILON)
     read = mixture * scale
     read_buf[0] = jnp.concatenate([read[g:g + 1] for g in range(GROUP)], axis=1).astype(jnp.bfloat16)
-    read_copy = pltpu.make_async_copy(read_buf, read_out, sem.at[3])
+    read_copy = pltpu.make_async_copy(read_buf, read_out, sem.at[2])
     read_copy.start()
-    for kind, cache in enumerate((k_out, v_out)):
-        pltpu.make_async_copy(cache, cache, sem.at[kind]).wait()
+    caches = land.at[:, pl.ds(0, 2 * block)]
+    pltpu.make_async_copy(caches, caches, sem.at[0]).wait()
     off_copy.wait()
     read_copy.wait()
 
@@ -384,7 +384,7 @@
         out_specs=(hbm,) * len(outs),
         scratch_shapes=[
             pltpu.VMEM(*read),
-            pltpu.SemaphoreType.DMA((len(outs),)),
+            pltpu.SemaphoreType.DMA((3,)),
         ],
         compiler_params=pltpu.CompilerParams(vmem_limit_bytes=WRITE_BYTES),
     )(*held)

time: 22.6 us -> 22.6 us (level)
  no operation moved by 1% of the time
where the time goes in v5:
time: 22.6 us; the launch traced here: 22.5 us
  Pallas kernels  21.8 us (96%)
  between operations  0.64 us (3%)
    pallas_call x1, Pallas kernels, shards(): pl.pallas_call(functools.partial(kernel, n, seqs, chunks), out_shape=tupl...  20.9 us
    pallas_call x1, Pallas kernels, shards(): pl.pallas_call(functools.partial(finish, n), out_shape=tuple((jax.ShapeDt...  0.91 us

profile of v5, /device:TPU:8, one launch (start us, length us, event | category | flops | bytes accessed | tf_op | source)
XLA Modules:
  0.0 22.5 jit_solution(16693651832270032986)
XLA Ops:
  0.6 20.9 %shard_map.102 = (bf16[4,776,128]{2,1,0:T(8,128)(2,1)S(1)}, bf16[1,1,1536]{2,1,0:T(2,128)(2,1)S(1)}, f32[8,1536]{1,0:T(8,128)S(1)}, f32[8,128]{1,0:T(8,128)S(1)}) custom-call(bf16[384,2048]{1,0:T(8,128)(2,1)} %bitcast.4, f32[1,2048]{1,0:T(1,128)} %bitcast.5, bf16[2048,512]{1,0:T(8,128)(2,1)} %wk_hbm.1, bf16[2048,512]{1,0:T(8,128)(2,1)} %wv_hbm.1, ...), custom_call_target="tpu_custom_call" | custom-call | tf_op jit(solution)/shard_map/pallas_call | solution.py:346
  21.6 0.9 %shard_map.103 = (bf16[1,1,1536,128]{3,2,1,0:T(8,128)(2,1)}, bf16[1,1,1536,128]{3,2,1,0:T(8,128)(2,1)}, bf16[1,1,1536]{2,1,0:T(2,128)(2,1)}, bf16[1,1,512]{2,1,0:T(2,128)(2,1)}) custom-call(bf16[4,776,128]{2,1,0:T(8,128)(2,1)S(1)} %get-tuple-element.8.land, bf16[1,1,1536]{2,1,0:T(2,128)(2,1)S(1)} %get-tuple-element.9.off_in, ...), custom_call_target="tpu_custom_call" | custom-call | tf_op jit(solution)/shard_map/pallas_call | solution.py:380

commit v6 on v5

--- a/solution.py
+++ b/solution.py
@@ -34,7 +34,7 @@
 def kernel(
     n, seqs, chunks, x_hbm, gain_hbm, wk_hbm, wv_hbm, off_hbm, bias_hbm, q_hbm,
     land, off_out, stick, mix_out,
-    x_buf, scaled, row_scale, weights, sends, gain_buf, bias_buf, off_in, off_tiles, q_buf,
+    x_buf, normed, weights, sends, gain_buf, bias_buf, off_in, off_tiles, q_buf,
     x_sem, w_sem, small_sem, land_sem,
 ):
     total, width = x_buf.shape
@@ -98,9 +98,8 @@
         def step(i, _):
             rows = pl.ds(pl.multiple_of(start + i * STEP, STEP), STEP)
             x = x_buf[rows, :].astype(jnp.float32)
-            scaled[rows, :] = (x * gain).astype(jnp.bfloat16)
             scale = lax.rsqrt(jnp.mean(x * x, axis=-1, keepdims=True) + EPSILON)
-            row_scale[rows, :] = jnp.broadcast_to(scale, (STEP, HD))
+            normed[rows, :] = (x * scale * gain).astype(jnp.bfloat16)
             return 0
 
         lax.fori_loop(0, count // STEP, step, 0, unroll=4)
@@ -126,34 +125,32 @@
         base = lax.div(peer(i), KVH) * block if seqs > 1 else 0
         rows = pl.ds(pl.multiple_of(base + start, STEP) if seqs > 1 else start, count)
         product = jnp.dot(
-            scaled[rows, :], weights[slot(i), :, columns], preferred_element_type=jnp.float32
+            normed[rows, :], weights[slot(i), :, columns], preferred_element_type=jnp.float32
         )
-        scale = row_scale[rows, :]
         return [
-            (product[:, c:c + HD] * scale).astype(jnp.bfloat16)
-            for c in range(0, product.shape[1], HD)
+            product[:, c:c + HD].astype(jnp.bfloat16) for c in range(0, product.shape[1], HD)
         ]
 
     def prepare_and_project(start, count, columns):
         rows = pl.ds(start, count)
+        squares = jnp.zeros((count, HD), jnp.float32)
+        for c in range(0, width, HD):
+            x = x_buf[rows, pl.ds(c, HD)].astype(jnp.float32)
+            squares = squares + x * x
+        scale = lax.rsqrt(jnp.sum(squares, axis=-1, keepdims=True) / width + EPSILON)
+        if start == 0:
+            w_copies[0].wait()
         product = jnp.zeros((count, columns.size), jnp.float32)
-        squares = jnp.zeros((count, HD), jnp.float32)
         for k in range(0, width, DEPTH):
             part = pl.ds(k, DEPTH)
             x = x_buf[rows, part].astype(jnp.float32)
-            y = (x * gain[:, k:k + DEPTH]).astype(jnp.bfloat16)
-            scaled[rows, part] = y
-            for c in range(0, DEPTH, HD):
-                squares = squares + x[:, c:c + HD] * x[:, c:c + HD]
+            y = (x * scale * gain[:, k:k + DEPTH]).astype(jnp.bfloat16)
+            normed[rows, part] = y
             product = product + jnp.dot(
                 y, weights[slot(1), part, columns], preferred_element_type=jnp.float32
             )
-        scale = lax.rsqrt(jnp.sum(squares, axis=-1, keepdims=True) / width + EPSILON)
-        scale = jnp.broadcast_to(scale, (count, HD))
-        row_scale[rows, :] = scale
         return [
-            (product[:, c:c + HD] * scale).astype(jnp.bfloat16)
-            for c in range(0, columns.size, HD)
+            product[:, c:c + HD].astype(jnp.bfloat16) for c in range(0, columns.size, HD)
         ]
 
     def remote(src, dst, landed, target):
@@ -198,7 +195,6 @@
                 later_loads()
             keys, values = pl.ds(start, count), pl.ds(block + start, count)
             if c == 0:
-                w_copies[0].wait()
                 sends[0, keys], = prepare_and_project(start, count, pl.ds(0, HD))
                 pl.semaphore_wait(barrier, n - 1)
                 copy_out(1, keys)
@@ -351,7 +347,6 @@
         scratch_shapes=[
             pltpu.VMEM((total, width), jnp.bfloat16),
             pltpu.VMEM((total, width), jnp.bfloat16),
-            pltpu.VMEM((total, HD), jnp.float32),
             pltpu.VMEM((KVH, width, 2 * HD), jnp.bfloat16),
             pltpu.VMEM((n - 1, unit, HD), jnp.bfloat16),
             pltpu.VMEM((1, width), jnp.float32),

time: 22.6 us -> 22.8 us (level)
  no operation moved by 1% of the time
where the time goes in v6:
time: 22.8 us; the launch traced here: 22.6 us
  Pallas kernels  22 us (96%)
  between operations  0.64 us (3%)
    pallas_call x1, Pallas kernels, shards(): pl.pallas_call(functools.partial(kernel, n, seqs, chunks), out_shape=tupl...  21 us
    pallas_call x1, Pallas kernels, shards(): pl.pallas_call(functools.partial(finish, n), out_shape=tuple((jax.ShapeDt...  0.91 us

profile of v6, /device:TPU:8, one launch (start us, length us, event | category | flops | bytes accessed | tf_op | source)
XLA Modules:
  0.0 22.6 jit_solution(5594948949621236976)
XLA Ops:
  0.6 21.0 %shard_map.102 = (bf16[4,776,128]{2,1,0:T(8,128)(2,1)S(1)}, bf16[1,1,1536]{2,1,0:T(2,128)(2,1)S(1)}, f32[8,1536]{1,0:T(8,128)S(1)}, f32[8,128]{1,0:T(8,128)S(1)}) custom-call(bf16[384,2048]{1,0:T(8,128)(2,1)} %bitcast.4, f32[1,2048]{1,0:T(1,128)} %bitcast.5, bf16[2048,512]{1,0:T(8,128)(2,1)} %wk_hbm.1, bf16[2048,512]{1,0:T(8,128)(2,1)} %wv_hbm.1, ...), custom_call_target="tpu_custom_call" | custom-call | tf_op jit(solution)/shard_map/pallas_call | solution.py:342
  21.7 0.9 %shard_map.103 = (bf16[1,1,1536,128]{3,2,1,0:T(8,128)(2,1)}, bf16[1,1,1536,128]{3,2,1,0:T(8,128)(2,1)}, bf16[1,1,1536]{2,1,0:T(2,128)(2,1)}, bf16[1,1,512]{2,1,0:T(2,128)(2,1)}) custom-call(bf16[4,776,128]{2,1,0:T(8,128)(2,1)S(1)} %get-tuple-element.8.land, bf16[1,1,1536]{2,1,0:T(2,128)(2,1)S(1)} %get-tuple-element.9.off_in, ...), custom_call_target="tpu_custom_call" | custom-call | tf_op jit(solution)/shard_map/pallas_call | solution.py:375

commit v7 on v5

--- a/solution.py
+++ b/solution.py
@@ -16,7 +16,7 @@
 ROWS = 128
 STEP = 16
 TILE = 8
-DEPTH = 256
+DEPTH = 1024
 VMEM_BYTES = 67043328
 SPARE_BYTES = 524288
 WRITE_BYTES = 1048576

time: 22.6 us -> 22.6 us (level)
  no operation moved by 1% of the time
where the time goes in v7:
time: 22.6 us; the launch traced here: 22.5 us
  Pallas kernels  21.8 us (96%)
  between operations  0.64 us (3%)
    pallas_call x1, Pallas kernels, shards(): pl.pallas_call(functools.partial(kernel, n, seqs, chunks), out_shape=tupl...  20.9 us
    pallas_call x1, Pallas kernels, shards(): pl.pallas_call(functools.partial(finish, n), out_shape=tuple((jax.ShapeDt...  0.91 us

profile of v7, /device:TPU:8, one launch (start us, length us, event | category | flops | bytes accessed | tf_op | source)
XLA Modules:
  0.0 22.5 jit_solution(17462786541226816537)
XLA Ops:
  0.6 20.9 %shard_map.102 = (bf16[4,776,128]{2,1,0:T(8,128)(2,1)S(1)}, bf16[1,1,1536]{2,1,0:T(2,128)(2,1)S(1)}, f32[8,1536]{1,0:T(8,128)S(1)}, f32[8,128]{1,0:T(8,128)S(1)}) custom-call(bf16[384,2048]{1,0:T(8,128)(2,1)} %bitcast.4, f32[1,2048]{1,0:T(1,128)} %bitcast.5, bf16[2048,512]{1,0:T(8,128)(2,1)} %wk_hbm.1, bf16[2048,512]{1,0:T(8,128)(2,1)} %wv_hbm.1, ...), custom_call_target="tpu_custom_call" | custom-call | tf_op jit(solution)/shard_map/pallas_call | solution.py:346
  21.6 0.9 %shard_map.103 = (bf16[1,1,1536,128]{3,2,1,0:T(8,128)(2,1)}, bf16[1,1,1536,128]{3,2,1,0:T(8,128)(2,1)}, bf16[1,1,1536]{2,1,0:T(2,128)(2,1)}, bf16[1,1,512]{2,1,0:T(2,128)(2,1)}) custom-call(bf16[4,776,128]{2,1,0:T(8,128)(2,1)S(1)} %get-tuple-element.8.land, bf16[1,1,1536]{2,1,0:T(2,128)(2,1)S(1)} %get-tuple-element.9.off_in, ...), custom_call_target="tpu_custom_call" | custom-call | tf_op jit(solution)/shard_map/pallas_call | solution.py:380
